TPU v7x, 32 devices: a whole 2x2x4 slice. The times are simulated.
32 devices in a mesh: sp: 8 (over z, x), tp: 4 (over y, core).
Axes of the slice: x: 2, y: 2, z: 4, core: 2. Of those that a mesh axis runs over, the one named last changes fastest.
Arguments:
- tokens: bfloat16 [2048, 2048], P(('sp', 'tp')), may hold values from -6 to 6
- norm_gain: float32 [2048], replicated, may hold values from 0.1 to 1.9
- w_glu_a: bfloat16 [2048, 2048], P(None, 'tp'), may hold values from -0.125 to 0.125
- w_glu_b: bfloat16 [2048, 2048], P(None, 'tp'), may hold values from -0.125 to 0.125
- conv_taps: float32 [31, 2048], P(None, 'tp'), may hold values from -6 to 6
- ln_gain: float32 [2048], P('tp'), may hold values from 0.1 to 1.9
- w_query: bfloat16 [2048, 2048], P(None, 'tp'), may hold values from -0.125 to 0.125
- w_key: bfloat16 [2048, 512], P(None, 'tp'), may hold values from -0.125 to 0.125
- w_value: bfloat16 [2048, 512], P(None, 'tp'), may hold values from -0.125 to 0.125
- query_gain: float32 [16, 128], P('tp'), may hold values from 1 to 40
- key_gain: float32 [4, 128], P('tp'), may hold values from 0.1 to 1.9
- lam_head: float32 [16], P('tp'), may hold values from 0.3 to 0.8
- sub_gain: float32 [128], replicated, may hold values from 0.1 to 1.9
- w_out_conv: bfloat16 [2048, 2048], P('tp'), may hold values from -0.09375 to 0.09375
- w_out_attn: bfloat16 [2048, 2048], P('tp'), may hold values from -0.09375 to 0.09375
Outputs:
- mixed: bfloat16 [2048, 2048], P(('sp', 'tp'))
- log_sums: float32 [2, 16, 2048], P(None, 'tp', 'sp')
All inputs are finite; a program needn't handle non-finite values.
Results may differ from a plain program's by a relative error of at most 0.015.
The roundings to bfloat16 on the way count: a program that leaves them out, or rounds other values in their place, can miss the bound.
Values may be sent and summed in bfloat16 or wider, within the bound.
A program may use at most 128 MiB of HBM per device.

v0:
```python
import functools

import jax
import jax.numpy as jnp
from jax import lax
from jax.experimental import pallas as pl
from jax.experimental.pallas import tpu as pltpu
from jax.sharding import PartitionSpec as P

KW = 31
HALO = 32
F32 = jnp.float32
BF16 = jnp.bfloat16
MESH = pl.DeviceIdType.MESH


def dot(a, b):
    return jnp.dot(a, b, preferred_element_type=F32)


def kernel(
    sp_n,
    tp_n,
    tokens,
    norm_gain,
    w_glu_a,
    w_glu_b,
    taps,
    ln_gain,
    w_query,
    w_key,
    w_value,
    q_gain,
    k_gain,
    lam,
    sub_gain,
    w_out_conv,
    w_out_attn,
    mixed,
    logs,
    wa,
    wb,
    wq,
    wkv,
    woc,
    woa,
    nrm,
    kv,
    qtz,
    gat,
    halo_s,
    halo_r,
    conv,
    st,
    stat,
    c_out,
    m_ref,
    l_ref,
    acc,
    a_out,
    part,
    mate_s,
    mate_r,
    y_s,
    y_r,
    w_sem,
    ag_send,
    ag_recv,
    z_send,
    x_send,
    kv_recv,
    halo_sem,
    stat_send,
    stat_recv,
    mate_send,
    mate_recv,
    y_send,
    y_recv,
):
    sp = lax.axis_index("sp")
    tp = lax.axis_index("tp")
    rows = tokens.shape[0]
    width = tokens.shape[1]
    tok = rows * tp_n
    half_rows = tok // 2
    heads = q_gain.shape[0]
    vdim = sub_gain.shape[1]
    hd = q_gain.shape[1] // 2
    chans = taps.shape[1]
    core = tp % 2
    y = tp // 2
    yo = 1 - y
    mate = tp + 1 - 2 * core
    cross = (tp + 2) % 4
    lane = sp % 2
    pos = sp // 2
    npos = sp_n // 2
    xmate = sp + 1 - 2 * lane

    bar = pltpu.get_barrier_semaphore()

    def greet_sp(i, c):
        pl.semaphore_signal(bar, inc=1, device_id=((sp + i) % sp_n, tp), device_id_type=MESH)
        return c

    lax.fori_loop(1, sp_n, greet_sp, 0)
    for i in range(1, tp_n):
        pl.semaphore_signal(bar, inc=1, device_id=(sp, (tp + i) % tp_n), device_id_type=MESH)

    kw = w_key.shape[1]
    loads = [
        pltpu.make_async_copy(w_key, wkv.at[:, :kw], w_sem.at[0]),
        pltpu.make_async_copy(w_value, wkv.at[:, kw:], w_sem.at[1]),
        pltpu.make_async_copy(w_glu_a, wa, w_sem.at[2]),
        pltpu.make_async_copy(w_glu_b, wb, w_sem.at[3]),
        pltpu.make_async_copy(w_query, wq, w_sem.at[4]),
        pltpu.make_async_copy(w_out_conv, woc, w_sem.at[5]),
        pltpu.make_async_copy(w_out_attn, woa, w_sem.at[6]),
    ]
    for copy in loads:
        copy.start()

    x = tokens[...].astype(F32)
    scale = lax.rsqrt(jnp.mean(x * x, axis=-1, keepdims=True) + 1e-06)
    nrm[tp] = (x * scale * norm_gain[...]).astype(BF16)
    qtz[...] = jnp.zeros_like(qtz)
    pl.semaphore_wait(bar, sp_n - 1 + tp_n - 1)

    ag_chunks = 4

    def ag_copy(slot, k, i, target):
        piece = pl.ds(i * (rows // ag_chunks), rows // ag_chunks)
        return pltpu.make_async_remote_copy(
            src_ref=nrm.at[slot, piece],
            dst_ref=nrm.at[slot, piece],
            send_sem=ag_send.at[k, i],
            recv_sem=ag_recv.at[k, i],
            device_id=(sp, target),
            device_id_type=MESH,
        )

    ag_cross = [ag_copy(tp, 0, i, cross) for i in range(ag_chunks)]
    ag_mate = [
        pltpu.make_async_remote_copy(
            src_ref=nrm.at[tp],
            dst_ref=nrm.at[tp],
            send_sem=ag_send.at[1, 0],
            recv_sem=ag_recv.at[1, 0],
            device_id=(sp, mate),
            device_id_type=MESH,
        )
    ]
    ag_fwd = [ag_copy(cross, 2, i, mate) for i in range(ag_chunks)]
    for copy in ag_cross + ag_mate:
        copy.start()

    def half_in(h):
        return nrm[pl.ds(2 * h, 2)].reshape(half_rows, width)

    def proj_kv(h):
        res = dot(half_in(h), wkv[...])
        k = res[:, :kw]
        v = res[:, kw:]
        first = lax.broadcasted_iota(jnp.int32, k.shape, 1) < hd
        sq = k * k
        s0 = jnp.sum(jnp.where(first, sq, 0.0), axis=1, keepdims=True)
        s1 = jnp.sum(jnp.where(first, 0.0, sq), axis=1, keepdims=True)
        r = jnp.where(first, lax.rsqrt(s0 / hd + 1e-06), lax.rsqrt(s1 / hd + 1e-06))
        kv[sp, h, :half_rows, :] = (k * r * k_gain[...]).astype(BF16)
        kv[sp, h, half_rows:, :] = v.T.astype(BF16)

    def z_copy(t, h):
        return pltpu.make_async_remote_copy(
            src_ref=kv.at[sp, h],
            dst_ref=kv.at[sp, h],
            send_sem=z_send.at[t, h],
            recv_sem=kv_recv.at[sp, h],
            device_id=(t * 2 + lane, tp),
            device_id_type=MESH,
        )

    def x_copy(p, h):
        s = p * 2 + lane
        return pltpu.make_async_remote_copy(
            src_ref=kv.at[s, h],
            dst_ref=kv.at[s, h],
            send_sem=x_send.at[p, h],
            recv_sem=kv_recv.at[s, h],
            device_id=(xmate, tp),
            device_id_type=MESH,
        )

    def arrived(s, h):
        pltpu.make_async_remote_copy(
            src_ref=kv.at[s, h],
            dst_ref=kv.at[s, h],
            send_sem=x_send.at[0, h],
            recv_sem=kv_recv.at[s, h],
            device_id=(xmate, tp),
            device_id_type=MESH,
        ).wait_recv()

    def send_kv(h):
        @pl.when(lane == 0)
        def _():
            x_copy(pos, h).start()

        def one(i, c):
            z_copy(npos - 1 - i, h).start()
            return c

        lax.fori_loop(0, npos - 1 - pos, one, 0)

    def relay_kv(h):
        def one(i, c):
            p = pos - 1 - i
            arrived(p * 2 + lane, h)
            x_copy(p, h).start()
            return c

        lax.fori_loop(0, pos, one, 0)

    def proj_glu(h):
        xin = half_in(h)
        wide = 256

        def one(n, c):
            cols = pl.ds(pl.multiple_of(n * wide, wide), wide)
            a = dot(xin, wa[:, cols])
            b = dot(xin, wb[:, cols])
            g = (a * jax.nn.sigmoid(b)).astype(BF16)
            gat[pl.ds(pl.multiple_of(HALO + h * half_rows, HALO), half_rows), cols] = g.astype(F32)

            @pl.when(h == 1)
            def _():
                halo_s[:, cols] = g[half_rows - HALO :, :]

            return c

        lax.fori_loop(0, chans // wide, one, 0)

    def proj_q(h):
        xin = half_in(h)

        def one(n, c):
            q = dot(xin, wq[:, pl.ds(pl.multiple_of(n * 4 * hd, 4 * hd), 4 * hd)])
            qt = q.T.reshape(4, hd, half_rows)
            r = lax.rsqrt(jnp.mean(qt * qt, axis=1, keepdims=True) + 1e-06)
            qn = qt * r
            for j in range(2):
                gain = jnp.broadcast_to(q_gain[pl.ds(n * 2 + j, 1), :], (2 * hd, 2 * hd)).T
                for m in range(2):
                    gm = gain[m * hd : (m + 1) * hd, :half_rows]
                    val = (qn[j * 2 + m] * gm * hd ** (-0.5)).astype(BF16)
                    first = (n * 2 + j) * tok + m * half_rows
                    lanes = pl.ds(pl.multiple_of(first, half_rows), half_rows)
                    qtz[h, m * hd : (m + 1) * hd, lanes] = val
            return c

        lax.fori_loop(0, heads // 2, one, 0)

    def halo_copy():
        return pltpu.make_async_remote_copy(
            src_ref=halo_s,
            dst_ref=halo_r,
            send_sem=halo_sem.at[0],
            recv_sem=halo_sem.at[1],
            device_id=((sp + 1) % sp_n, tp),
            device_id_type=MESH,
        )

    def send_halo(h):
        @pl.when((sp < sp_n - 1) & (h == 1))
        def _():
            halo_copy().start()

    loads[0].wait()
    loads[1].wait()
    ag_mate[0].wait_recv()
    proj_kv(y)
    send_kv(y)
    loads[2].wait()
    loads[3].wait()
    proj_glu(y)
    send_halo(y)
    loads[4].wait()
    proj_q(y)
    for i in range(ag_chunks):
        ag_cross[i].wait_recv()
        ag_fwd[i].start()
    relay_kv(y)
    for i in range(ag_chunks):
        ag_fwd[i].wait_recv()
    proj_kv(yo)
    send_kv(yo)
    proj_glu(yo)
    send_halo(yo)
    proj_q(yo)

    def attend(blocks, q, diag):
        keys = jnp.concatenate(
            [kv[s, i, :half_rows, :] for s in blocks for i in range(2)], axis=0
        )
        vals = jnp.concatenate(
            [kv[s, i, half_rows:, :] for s in blocks for i in range(2)], axis=1
        )
        if diag:
            kpos = lax.broadcasted_iota(jnp.int32, (tok, tok), 0)
            qpos = lax.broadcasted_iota(jnp.int32, (tok, tok), 1)
            qpos = jnp.where(qpos >= half_rows, qpos - half_rows, qpos) + q * half_rows
            seen = kpos <= qpos
        every = dot(keys, qtz[q])
        for h in range(heads):
            sc = every[:, h * tok : (h + 1) * tok]
            if diag:
                sc = jnp.where(seen, sc, -1e30)
                top = jnp.max(sc, axis=0, keepdims=True)
                wgt = jnp.exp(sc - top)
                l_ref[h][q] = jnp.sum(wgt, axis=0, keepdims=True)
                acc[h][q] = dot(vals, wgt.astype(BF16))
            else:
                old = m_ref[h][q]
                top = jnp.maximum(old, jnp.max(sc, axis=0, keepdims=True))
                wgt = jnp.exp(sc - top)
                alpha = jnp.exp(old - top)
                l_ref[h][q] = l_ref[h][q] * alpha + jnp.sum(wgt, axis=0, keepdims=True)
                acc[h][q] = acc[h][q] * alpha + dot(vals, wgt.astype(BF16))
            m_ref[h][q] = top

    def own_block(q, c):
        attend([sp], q, True)
        return c

    lax.fori_loop(0, 2, own_block, 0)

    @pl.when(sp > 0)
    def _():
        halo_copy().wait_recv()
        gat[:HALO, :] = halo_r[...].astype(F32)

    @pl.when(sp == 0)
    def _():
        gat[:HALO, :] = jnp.zeros((HALO, chans), F32)

    st[...] = jnp.zeros_like(st)
    step_rows = 64

    def conv_cols(cc, c):
        cols = pl.ds(pl.multiple_of(cc * 128, 128), 128)
        for r0 in range(0, tok, step_rows):
            total = jnp.zeros((step_rows, 128), F32)
            for j in range(KW):
                total = total + taps[j : j + 1, cols] * gat[r0 + HALO - KW + 1 + j : r0 + HALO - KW + 1 + j + step_rows, cols]
            conv[r0 : r0 + step_rows, cols] = total
            st[0, r0 : r0 + step_rows, :] += total
            st[1, r0 : r0 + step_rows, :] += total * total
        return c

    lax.fori_loop(0, chans // 128, conv_cols, 0)
    stat[tp] = jnp.concatenate(
        [jnp.sum(st[i].T, axis=0, keepdims=True) for i in range(2)], axis=0
    )

    def stat_copy(i):
        return pltpu.make_async_remote_copy(
            src_ref=stat.at[tp],
            dst_ref=stat.at[tp],
            send_sem=stat_send.at[i],
            recv_sem=stat_recv.at[i],
            device_id=(sp, (tp + i) % tp_n),
            device_id_type=MESH,
        )

    for i in range(1, tp_n):
        stat_copy(i).start()
    relay_kv(yo)

    @pl.when(lane == 1)
    def _():
        arrived(sp - 1, y)
        arrived(sp - 1, yo)

        def partner_block(q, c):
            attend([sp - 1], q, False)
            return c

        lax.fori_loop(0, 2, partner_block, 0)

    for i in range(1, tp_n):
        stat_copy(i).wait_recv()
    sums = stat[0]
    for i in range(1, tp_n):
        sums = sums + stat[i]
    sums = sums / (chans * tp_n)
    mu = sums[0:1]
    inv = lax.rsqrt(sums[1:2] - mu * mu + 1e-05)
    mu_t = jnp.broadcast_to(mu, (128, tok)).T
    inv_t = jnp.broadcast_to(inv, (128, tok)).T
    for cc in range(0, chans, 128):
        val = (conv[:, cc : cc + 128] - mu_t) * inv_t * ln_gain[:, cc : cc + 128]
        c_out[:, cc : cc + 128] = (val * jax.nn.sigmoid(val)).astype(BF16)
    loads[5].wait()
    wide = y_s.shape[2]
    chunks = width // wide

    def out_conv(n, c):
        cols = pl.ds(pl.multiple_of(n * wide, wide), wide)
        part[:, cols] = dot(c_out[...], woc[:, cols])
        return c

    lax.fori_loop(0, chunks, out_conv, 0)

    def pairs(q, first):
        def one(i, c):
            p = pos - 1 - i
            if first:
                arrived(p * 2 + 1 - lane, y)
                arrived(p * 2 + 1 - lane, yo)
            attend([p * 2, p * 2 + 1], q, False)
            return c

        lax.fori_loop(0, pos, one, 0)

    sub_t = jnp.broadcast_to(sub_gain[...], (half_rows, vdim)).T

    def close_heads(q):
        at = pl.ds(pl.multiple_of(q * half_rows, half_rows), half_rows)
        for h in range(heads):
            total = l_ref[h][q]
            log_row = m_ref[h][q] + jnp.log(total)
            maps = acc[h][q] / total
            for m in range(2):
                logs[m, h : h + 1, at] = log_row[:, m * half_rows : (m + 1) * half_rows]
            diff = maps[:, :half_rows] - lam[h] * maps[:, half_rows:]
            out = diff * lax.rsqrt(jnp.mean(diff * diff, axis=0, keepdims=True) + 1e-06) * sub_t
            a_out[at, h * vdim : (h + 1) * vdim] = out.T.astype(BF16)

    loads[6].wait()

    def mate_copy(k, n):
        return pltpu.make_async_remote_copy(
            src_ref=mate_s.at[k, n],
            dst_ref=mate_r.at[k, n],
            send_sem=mate_send.at[k, n],
            recv_sem=mate_recv.at[k, n],
            device_id=(sp, mate),
            device_id_type=MESH,
        )

    def y_copy(n):
        return pltpu.make_async_remote_copy(
            src_ref=y_s.at[n],
            dst_ref=y_r.at[n],
            send_sem=y_send.at[n],
            recv_sem=y_recv.at[n],
            device_id=(sp, cross),
            device_id_type=MESH,
        )

    def half_of(h):
        return pl.ds(pl.multiple_of(h * half_rows, half_rows), half_rows)

    def owner_rows(h, c):
        return pl.ds(pl.multiple_of((h * 2 + c) * rows, rows), rows)

    def out_attn(k, h):
        def one(n, c):
            cols = pl.ds(pl.multiple_of(n * wide, wide), wide)
            part[half_of(h), cols] += dot(a_out[half_of(h), :], woa[:, cols])
            mate_s[k, n] = part[owner_rows(h, 1 - core), cols].astype(BF16)
            mate_copy(k, n).start()
            return c

        lax.fori_loop(0, chunks, one, 0)

    pairs(yo, True)
    close_heads(yo)
    out_attn(0, yo)

    def forward(n, c):
        cols = pl.ds(pl.multiple_of(n * wide, wide), wide)
        mate_copy(0, n).wait_recv()
        y_s[n] = (part[owner_rows(yo, core), cols] + mate_r[0, n].astype(F32)).astype(BF16)
        y_copy(n).start()
        return c

    lax.fori_loop(0, chunks, forward, 0)
    pairs(y, False)
    close_heads(y)
    out_attn(1, y)

    def finish(n, c):
        cols = pl.ds(pl.multiple_of(n * wide, wide), wide)
        mate_copy(1, n).wait_recv()
        y_copy(n).wait_recv()
        total = part[owner_rows(y, core), cols] + mate_r[1, n].astype(F32) + y_r[n].astype(F32)
        mixed[:, cols] = total.astype(BF16)
        return c

    lax.fori_loop(0, chunks, finish, 0)

    for copy in ag_cross + ag_mate + ag_fwd:
        copy.wait_send()
    for i in range(1, tp_n):
        stat_copy(i).wait_send()

    @pl.when(sp < sp_n - 1)
    def _():
        halo_copy().wait_send()

    for h in range(2):

        @pl.when(lane == 0)
        def _():
            x_copy(pos, h).wait_send()

        def z_done(i, c):
            z_copy(npos - 1 - i, h).wait_send()
            return c

        lax.fori_loop(0, npos - 1 - pos, z_done, 0)

        def x_done(i, c):
            x_copy(i, h).wait_send()
            return c

        lax.fori_loop(0, pos, x_done, 0)

    def rs_done(n, c):
        mate_copy(0, n).wait_send()
        mate_copy(1, n).wait_send()
        y_copy(n).wait_send()
        return c

    lax.fori_loop(0, chunks, rs_done, 0)


def on_device(sp_n, tp_n, *args):
    (
        tokens,
        norm_gain,
        w_glu_a,
        w_glu_b,
        conv_taps,
        ln_gain,
        w_query,
        w_key,
        w_value,
        query_gain,
        key_gain,
        lam_head,
        sub_gain,
        w_out_conv,
        w_out_attn,
    ) = args
    rows, width = tokens.shape
    tok = rows * tp_n
    half = tok // 2
    chans = conv_taps.shape[1]
    heads = lam_head.shape[0]
    qcols = w_query.shape[1]
    kcols = w_key.shape[1]
    vcols = w_value.shape[1]
    vdim = sub_gain.shape[0]
    acols = w_out_attn.shape[0]
    chunks = 4
    wide = width // chunks
    vmem = pl.BlockSpec(memory_space=pltpu.VMEM)
    anym = pl.BlockSpec(memory_space=pl.ANY)
    smem = pl.BlockSpec(memory_space=pltpu.SMEM)
    dma = pltpu.SemaphoreType.DMA
    return pl.pallas_call(
        functools.partial(kernel, sp_n, tp_n),
        out_shape=(
            jax.ShapeDtypeStruct((rows, width), BF16),
            jax.ShapeDtypeStruct((2, heads, tok), F32),
        ),
        in_specs=[vmem, vmem, anym, anym, vmem, vmem, anym, anym, anym, vmem, vmem, smem, vmem, anym, anym],
        out_specs=(vmem, vmem),
        scratch_shapes=[
            pltpu.VMEM((width, chans), BF16),
            pltpu.VMEM((width, chans), BF16),
            pltpu.VMEM((width, qcols), BF16),
            pltpu.VMEM((width, kcols + vcols), BF16),
            pltpu.VMEM((chans, width), BF16),
            pltpu.VMEM((acols, width), BF16),
            pltpu.VMEM((tp_n, rows, width), BF16),
            pltpu.VMEM((sp_n, 2, half + vcols, half), BF16),
            pltpu.VMEM((2, kcols, heads * tok), BF16),
            pltpu.VMEM((HALO + tok, chans), F32),
            pltpu.VMEM((HALO, chans), BF16),
            pltpu.VMEM((HALO, chans), BF16),
            pltpu.VMEM((tok, chans), F32),
            pltpu.VMEM((2, tok, 128), F32),
            pltpu.VMEM((tp_n, 2, tok), F32),
            pltpu.VMEM((tok, chans), BF16),
            [pltpu.VMEM((2, 1, tok), F32) for _ in range(heads)],
            [pltpu.VMEM((2, 1, tok), F32) for _ in range(heads)],
            [pltpu.VMEM((2, vdim, tok), F32) for _ in range(heads)],
            pltpu.VMEM((tok, acols), BF16),
            pltpu.VMEM((tok, width), F32),
            pltpu.VMEM((2, chunks, rows, wide), BF16),
            pltpu.VMEM((2, chunks, rows, wide), BF16),
            pltpu.VMEM((chunks, rows, wide), BF16),
            pltpu.VMEM((chunks, rows, wide), BF16),
            dma((7,)),
            dma((3, 4)),
            dma((3, 4)),
            dma((sp_n // 2, 2)),
            dma((sp_n // 2, 2)),
            dma((sp_n, 2)),
            dma((2,)),
            dma((tp_n,)),
            dma((tp_n,)),
            dma((2, chunks)),
            dma((2, chunks)),
            dma((chunks,)),
            dma((chunks,)),
        ],
        compiler_params=pltpu.CompilerParams(
            collective_id=0, has_side_effects=True, vmem_limit_bytes=56 * 2**20
        ),
    )(
        tokens,
        norm_gain.reshape(1, -1),
        w_glu_a,
        w_glu_b,
        conv_taps,
        ln_gain.reshape(1, -1),
        w_query,
        w_key,
        w_value,
        query_gain,
        key_gain,
        lam_head,
        sub_gain.reshape(1, -1),
        w_out_conv,
        w_out_attn,
    )


def solution(mesh):
    return jax.shard_map(
        functools.partial(on_device, mesh.shape["sp"], mesh.shape["tp"]),
        mesh=mesh,
        in_specs=(
            P(("sp", "tp"), None),
            P(),
            P(None, "tp"),
            P(None, "tp"),
            P(None, "tp"),
            P("tp"),
            P(None, "tp"),
            P(None, "tp"),
            P(None, "tp"),
            P("tp", None),
            P("tp", None),
            P("tp"),
            P(),
            P("tp", None),
            P("tp", None),
        ),
        out_specs=(P(("sp", "tp"), None), P(None, "tp", "sp")),
        check_vma=False,
    )
```

profile of v0, /device:TPU:25, one launch (start us, length us, event | category | flops | bytes accessed | tf_op | source)
XLA Modules:
  0.0 44.5 jit_solution(11024737141274532853)
XLA Ops:
  0.6 40.9 %shard_map.158 = (bf16[64,2048]{1,0:T(8,128)(2,1)}, f32[2,4,256]{2,1,0:T(4,128)}) custom-call(bf16[64,2048]{1,0:T(8,128)(2,1)} %tokens.1, f32[1,2048]{1,0:T(1,128)} %bitcast.3, bf16[2048,512]{1,0:T(8,128)(2,1)} %w_glu_a.1, bf16[2048,512]{1,0:T(8,128)(2,1)} %w_glu_b.1, f32[31,512]{1,0:T(8,128)} %taps.1, f32[1,512]{1,0:T(1,128)} %bitcast.4, ...), custom_call_target="tpu_custom_call" | custom-call | tf_op jit(solution)/shard_map/pallas_call | solution.py:572
  41.5 1.7 %copy.19 = bf16[64,2048]{1,0:T(8,128)(2,1)} copy(bf16[64,2048]{1,0:T(8,128)(2,1)} %get-tuple-element.4) | data formatting | bytes 524288
  43.2 1.3 %copy.20 = f32[2,4,256]{2,1,0:T(4,128)} copy(f32[2,4,256]{2,1,0:T(4,128)} %get-tuple-element.5) | data formatting | bytes 16384
where the time goes:
time: 45.2 us; the launch traced here: 44.5 us
  Pallas kernels  40.9 us (90%)
  local copies, waits for them, and re-layouts  2.96 us (7%)
  between operations  0.64 us (1%)
    pallas_call x1, Pallas kernels, on_device(): pl.pallas_call(functools.partial(kernel, sp_n, tp_n), out_shape=(jax.Shap...  40.9 us
    unnamed x2, local copies, waits for them, and re-layouts  2.96 us

commit v1 on v0

--- a/solution.py
+++ b/solution.py
@@ -21,23 +21,31 @@
 def kernel(
     sp_n,
     tp_n,
-    tokens,
-    norm_gain,
+    tokens_hbm,
+    norm_gain_hbm,
     w_glu_a,
     w_glu_b,
-    taps,
-    ln_gain,
+    taps_hbm,
+    ln_gain_hbm,
     w_query,
     w_key,
     w_value,
+    q_gain_hbm,
+    k_gain_hbm,
+    lam_hbm,
+    sub_gain_hbm,
+    w_out_conv,
+    w_out_attn,
+    mixed,
+    logs,
+    tokens,
+    norm_gain,
+    taps,
+    ln_gain,
     q_gain,
     k_gain,
     lam,
     sub_gain,
-    w_out_conv,
-    w_out_attn,
-    mixed,
-    logs,
     wa,
     wb,
     wq,
@@ -63,6 +71,7 @@
     mate_r,
     y_s,
     y_r,
+    in_sem,
     w_sem,
     ag_send,
     ag_recv,
@@ -108,6 +117,23 @@
         pl.semaphore_signal(bar, inc=1, device_id=(sp, (tp + i) % tp_n), device_id_type=MESH)
 
     kw = w_key.shape[1]
+    smalls = [
+        pltpu.make_async_copy(src, dst, in_sem.at[i])
+        for i, (src, dst) in enumerate(
+            [
+                (tokens_hbm, tokens),
+                (norm_gain_hbm, norm_gain),
+                (k_gain_hbm, k_gain),
+                (q_gain_hbm, q_gain),
+                (taps_hbm, taps),
+                (ln_gain_hbm, ln_gain),
+                (sub_gain_hbm, sub_gain),
+                (lam_hbm, lam),
+            ]
+        )
+    ]
+    for copy in smalls:
+        copy.start()
     loads = [
         pltpu.make_async_copy(w_key, wkv.at[:, :kw], w_sem.at[0]),
         pltpu.make_async_copy(w_value, wkv.at[:, kw:], w_sem.at[1]),
@@ -120,10 +146,12 @@
     for copy in loads:
         copy.start()
 
+    qtz[...] = jnp.zeros_like(qtz)
+    smalls[0].wait()
+    smalls[1].wait()
     x = tokens[...].astype(F32)
     scale = lax.rsqrt(jnp.mean(x * x, axis=-1, keepdims=True) + 1e-06)
     nrm[tp] = (x * scale * norm_gain[...]).astype(BF16)
-    qtz[...] = jnp.zeros_like(qtz)
     pl.semaphore_wait(bar, sp_n - 1 + tp_n - 1)
 
     ag_chunks = 4
@@ -274,6 +302,8 @@
         def _():
             halo_copy().start()
 
+    for copy in smalls[2:]:
+        copy.wait()
     loads[0].wait()
     loads[1].wait()
     ag_mate[0].wait_recv()
@@ -533,6 +563,17 @@
         return c
 
     lax.fori_loop(0, chunks, rs_done, 0)
+
+
+def put_out(mixed, logs, mixed_hbm, logs_hbm, sem):
+    copies = [
+        pltpu.make_async_copy(mixed, mixed_hbm, sem.at[0]),
+        pltpu.make_async_copy(logs, logs_hbm, sem.at[1]),
+    ]
+    for copy in copies:
+        copy.start()
+    for copy in copies:
+        copy.wait()
 
 
 def on_device(sp_n, tp_n, *args):
@@ -566,18 +607,25 @@
     chunks = 4
     wide = width // chunks
     vmem = pl.BlockSpec(memory_space=pltpu.VMEM)
-    anym = pl.BlockSpec(memory_space=pl.ANY)
-    smem = pl.BlockSpec(memory_space=pltpu.SMEM)
     dma = pltpu.SemaphoreType.DMA
-    return pl.pallas_call(
+    hbm = pl.BlockSpec(memory_space=pltpu.HBM)
+    mixed, logs = pl.pallas_call(
         functools.partial(kernel, sp_n, tp_n),
         out_shape=(
-            jax.ShapeDtypeStruct((rows, width), BF16),
-            jax.ShapeDtypeStruct((2, heads, tok), F32),
+            pltpu.VMEM((rows, width), BF16),
+            pltpu.VMEM((2, heads, tok), F32),
         ),
-        in_specs=[vmem, vmem, anym, anym, vmem, vmem, anym, anym, anym, vmem, vmem, smem, vmem, anym, anym],
+        in_specs=[hbm] * 15,
         out_specs=(vmem, vmem),
         scratch_shapes=[
+            pltpu.VMEM((rows, width), BF16),
+            pltpu.VMEM((1, width), F32),
+            pltpu.VMEM(conv_taps.shape, F32),
+            pltpu.VMEM((1, chans), F32),
+            pltpu.VMEM(query_gain.shape, F32),
+            pltpu.VMEM(key_gain.shape, F32),
+            pltpu.SMEM((heads,), F32),
+            pltpu.VMEM((1, vdim), F32),
             pltpu.VMEM((width, chans), BF16),
             pltpu.VMEM((width, chans), BF16),
             pltpu.VMEM((width, qcols), BF16),
@@ -603,6 +651,7 @@
             pltpu.VMEM((2, chunks, rows, wide), BF16),
             pltpu.VMEM((chunks, rows, wide), BF16),
             pltpu.VMEM((chunks, rows, wide), BF16),
+            dma((8,)),
             dma((7,)),
             dma((3, 4)),
             dma((3, 4)),
@@ -637,6 +686,19 @@
         w_out_conv,
         w_out_attn,
     )
+    return pl.pallas_call(
+        put_out,
+        out_shape=(
+            jax.ShapeDtypeStruct((rows, width), BF16),
+            jax.ShapeDtypeStruct((2, heads, tok), F32),
+        ),
+        in_specs=[vmem, vmem],
+        out_specs=(hbm, hbm),
+        scratch_shapes=[dma((2,))],
+    )(
+        pltpu.with_memory_space_constraint(mixed, pltpu.VMEM),
+        pltpu.with_memory_space_constraint(logs, pltpu.VMEM),
+    )
 
 
 def solution(mesh):

time: 45.2 us -> 41.2 us (0.912)
  local copies, waits for them, and re-layouts: 2.96 us -> 0 us
  Pallas kernels: 40.9 us -> 39.9 us
    unnamed x2 -> x0, local copies, waits for them, and re-layouts: 2.96 us -> none
    pallas_call x1 -> x2, Pallas kernels: 40.9 us -> 39.9 us  [the longest x1 39.1 us: on_device(): pl.pallas_call(functools.partial(kernel, sp_n, tp_n), out_shape=(pltpu.VM...]
where the time goes in v1:
time: 41.2 us; the launch traced here: 40.5 us
  Pallas kernels  39.9 us (97%)
  between operations  0.64 us (2%)
    pallas_call x1, Pallas kernels, on_device(): pl.pallas_call(functools.partial(kernel, sp_n, tp_n), out_shape=(pltpu.VM...  39.1 us

profile of v1, /device:TPU:25, one launch (start us, length us, event | category | flops | bytes accessed | tf_op | source)
XLA Modules:
  0.0 40.5 jit_solution(5444119057450302195)
XLA Ops:
  0.6 39.1 %shard_map.158 = (bf16[64,2048]{1,0:T(8,128)(2,1)S(1)}, f32[2,4,256]{2,1,0:T(4,128)S(1)}) custom-call(bf16[64,2048]{1,0:T(8,128)(2,1)} %tokens_hbm.1, f32[1,2048]{1,0:T(1,128)} %bitcast.3, bf16[2048,512]{1,0:T(8,128)(2,1)} %w_glu_a.1, bf16[2048,512]{1,0:T(8,128)(2,1)} %w_glu_b.1, f32[31,512]{1,0:T(8,128)} %taps_hbm.1, f32[1,512]{1,0:T(1,128)} %bitcast.4, ...), custom_call_target="tpu_custom_call" | custom-call | tf_op jit(solution)/shard_map/pallas_call | solution.py:612
  39.8 0.7 %shard_map.159 = (bf16[64,2048]{1,0:T(8,128)(2,1)}, f32[2,4,256]{2,1,0:T(4,128)}) custom-call(bf16[64,2048]{1,0:T(8,128)(2,1)S(1)} %get-tuple-element.4.mixed, f32[2,4,256]{2,1,0:T(4,128)S(1)} %get-tuple-element.5.logs), custom_call_target="tpu_custom_call" | custom-call | tf_op jit(solution)/shard_map/pallas_call | solution.py:689

commit v2 on v1

--- a/solution.py
+++ b/solution.py
@@ -71,7 +71,6 @@
     mate_r,
     y_s,
     y_r,
-    in_sem,
     w_sem,
     ag_send,
     ag_recv,
@@ -117,38 +116,37 @@
         pl.semaphore_signal(bar, inc=1, device_id=(sp, (tp + i) % tp_n), device_id_type=MESH)
 
     kw = w_key.shape[1]
-    smalls = [
-        pltpu.make_async_copy(src, dst, in_sem.at[i])
+    loads = [
+        pltpu.make_async_copy(src, dst, w_sem.at[i])
         for i, (src, dst) in enumerate(
             [
                 (tokens_hbm, tokens),
                 (norm_gain_hbm, norm_gain),
+                (w_key, wkv.at[:, :kw]),
+                (w_value, wkv.at[:, kw:]),
                 (k_gain_hbm, k_gain),
+                (w_glu_a, wa),
+                (w_glu_b, wb),
                 (q_gain_hbm, q_gain),
+                (w_query, wq),
                 (taps_hbm, taps),
                 (ln_gain_hbm, ln_gain),
+                (w_out_conv, woc),
                 (sub_gain_hbm, sub_gain),
                 (lam_hbm, lam),
+                (w_out_attn, woa),
             ]
         )
-    ]
-    for copy in smalls:
-        copy.start()
-    loads = [
-        pltpu.make_async_copy(w_key, wkv.at[:, :kw], w_sem.at[0]),
-        pltpu.make_async_copy(w_value, wkv.at[:, kw:], w_sem.at[1]),
-        pltpu.make_async_copy(w_glu_a, wa, w_sem.at[2]),
-        pltpu.make_async_copy(w_glu_b, wb, w_sem.at[3]),
-        pltpu.make_async_copy(w_query, wq, w_sem.at[4]),
-        pltpu.make_async_copy(w_out_conv, woc, w_sem.at[5]),
-        pltpu.make_async_copy(w_out_attn, woa, w_sem.at[6]),
     ]
     for copy in loads:
         copy.start()
 
+    def loaded(lo, hi):
+        for copy in loads[lo:hi]:
+            copy.wait()
+
     qtz[...] = jnp.zeros_like(qtz)
-    smalls[0].wait()
-    smalls[1].wait()
+    loaded(0, 2)
     x = tokens[...].astype(F32)
     scale = lax.rsqrt(jnp.mean(x * x, axis=-1, keepdims=True) + 1e-06)
     nrm[tp] = (x * scale * norm_gain[...]).astype(BF16)
@@ -257,7 +255,9 @@
             a = dot(xin, wa[:, cols])
             b = dot(xin, wb[:, cols])
             g = (a * jax.nn.sigmoid(b)).astype(BF16)
-            gat[pl.ds(pl.multiple_of(HALO + h * half_rows, HALO), half_rows), cols] = g.astype(F32)
+            at = pl.ds(pl.multiple_of(HALO + h * half_rows, HALO), half_rows)
+            for j in range(wide // 128):
+                gat[n * (wide // 128) + j, at, :] = g[:, j * 128 : (j + 1) * 128].astype(F32)
 
             @pl.when(h == 1)
             def _():
@@ -265,7 +265,8 @@
 
             return c
 
-        lax.fori_loop(0, chans // wide, one, 0)
+        for n in range(chans // wide):
+            one(n, 0)
 
     def proj_q(h):
         xin = half_in(h)
@@ -285,7 +286,8 @@
                     qtz[h, m * hd : (m + 1) * hd, lanes] = val
             return c
 
-        lax.fori_loop(0, heads // 2, one, 0)
+        for n in range(heads // 2):
+            one(n, 0)
 
     def halo_copy():
         return pltpu.make_async_remote_copy(
@@ -302,29 +304,25 @@
         def _():
             halo_copy().start()
 
-    for copy in smalls[2:]:
-        copy.wait()
-    loads[0].wait()
-    loads[1].wait()
+    loaded(2, 5)
     ag_mate[0].wait_recv()
     proj_kv(y)
     send_kv(y)
-    loads[2].wait()
-    loads[3].wait()
+    loaded(5, 7)
     proj_glu(y)
     send_halo(y)
-    loads[4].wait()
+    loaded(7, 9)
     proj_q(y)
     for i in range(ag_chunks):
         ag_cross[i].wait_recv()
         ag_fwd[i].start()
-    relay_kv(y)
     for i in range(ag_chunks):
         ag_fwd[i].wait_recv()
+    proj_glu(yo)
+    send_halo(yo)
     proj_kv(yo)
     send_kv(yo)
-    proj_glu(yo)
-    send_halo(yo)
+    relay_kv(y)
     proj_q(yo)
 
     def attend(blocks, q, diag):
@@ -357,88 +355,99 @@
                 acc[h][q] = acc[h][q] * alpha + dot(vals, wgt.astype(BF16))
             m_ref[h][q] = top
 
-    def own_block(q, c):
-        attend([sp], q, True)
-        return c
-
-    lax.fori_loop(0, 2, own_block, 0)
-
-    @pl.when(sp > 0)
-    def _():
-        halo_copy().wait_recv()
-        gat[:HALO, :] = halo_r[...].astype(F32)
-
-    @pl.when(sp == 0)
-    def _():
-        gat[:HALO, :] = jnp.zeros((HALO, chans), F32)
-
-    st[...] = jnp.zeros_like(st)
     step_rows = 64
-
-    def conv_cols(cc, c):
-        cols = pl.ds(pl.multiple_of(cc * 128, 128), 128)
-        for r0 in range(0, tok, step_rows):
-            total = jnp.zeros((step_rows, 128), F32)
-            for j in range(KW):
-                total = total + taps[j : j + 1, cols] * gat[r0 + HALO - KW + 1 + j : r0 + HALO - KW + 1 + j + step_rows, cols]
-            conv[r0 : r0 + step_rows, cols] = total
-            st[0, r0 : r0 + step_rows, :] += total
-            st[1, r0 : r0 + step_rows, :] += total * total
-        return c
-
-    lax.fori_loop(0, chans // 128, conv_cols, 0)
-    stat[tp] = jnp.concatenate(
-        [jnp.sum(st[i].T, axis=0, keepdims=True) for i in range(2)], axis=0
-    )
-
-    def stat_copy(i):
+    loaded(9, 10)
+
+    def conv_half(h):
+        @pl.when((h == 0) & (sp > 0))
+        def _():
+            halo_copy().wait_recv()
+            for j in range(chans // 128):
+                gat[j, :HALO, :] = halo_r[:, j * 128 : (j + 1) * 128].astype(F32)
+
+        @pl.when((h == 0) & (sp == 0))
+        def _():
+            gat[:, :HALO, :] = jnp.zeros((chans // 128, HALO, 128), F32)
+
+        st[...] = jnp.zeros_like(st)
+
+        def conv_cols(cc, c):
+            cols = pl.ds(pl.multiple_of(cc * 128, 128), 128)
+            rows_in = gat.at[cc, pl.ds(pl.multiple_of(h * half_rows, half_rows), HALO + half_rows), :]
+            rows_out = conv.at[cc, pl.ds(pl.multiple_of(h * half_rows, half_rows), half_rows), :]
+            for r0 in range(0, half_rows, step_rows):
+                total = jnp.zeros((step_rows, 128), F32)
+                for j in range(KW):
+                    first = r0 + HALO - KW + 1 + j
+                    total = total + taps[j : j + 1, cols] * rows_in[first : first + step_rows, :]
+                rows_out[r0 : r0 + step_rows, :] = total
+                st[0, r0 : r0 + step_rows, :] += total
+                st[1, r0 : r0 + step_rows, :] += total * total
+            return c
+
+        lax.fori_loop(0, chans // 128, conv_cols, 0)
+        stat[h, tp] = jnp.concatenate(
+            [jnp.sum(st[i].T, axis=0, keepdims=True) for i in range(2)], axis=0
+        )
+        for i in range(1, tp_n):
+            stat_copy(h, i).start()
+
+    def stat_copy(h, i):
         return pltpu.make_async_remote_copy(
-            src_ref=stat.at[tp],
-            dst_ref=stat.at[tp],
-            send_sem=stat_send.at[i],
-            recv_sem=stat_recv.at[i],
+            src_ref=stat.at[h, tp],
+            dst_ref=stat.at[h, tp],
+            send_sem=stat_send.at[h, i],
+            recv_sem=stat_recv.at[h, i],
             device_id=(sp, (tp + i) % tp_n),
             device_id_type=MESH,
         )
 
-    for i in range(1, tp_n):
-        stat_copy(i).start()
+    wide = y_s.shape[2]
+    chunks = width // wide
+
+    def half_of(h):
+        return pl.ds(pl.multiple_of(h * half_rows, half_rows), half_rows)
+
+    def close_conv(h):
+        for i in range(1, tp_n):
+            stat_copy(h, i).wait_recv()
+        sums = stat[h, 0]
+        for i in range(1, tp_n):
+            sums = sums + stat[h, i]
+        sums = sums / (chans * tp_n)
+        mu = sums[0:1]
+        inv = lax.rsqrt(sums[1:2] - mu * mu + 1e-05)
+        mu_t = jnp.broadcast_to(mu, (128, half_rows)).T
+        inv_t = jnp.broadcast_to(inv, (128, half_rows)).T
+        for cc in range(chans // 128):
+            cols = slice(cc * 128, (cc + 1) * 128)
+            val = (conv[cc, half_of(h), :] - mu_t) * inv_t * ln_gain[:, cols]
+            c_out[half_of(h), cols] = (val * jax.nn.sigmoid(val)).astype(BF16)
+
+    def out_conv(h):
+        for n in range(chunks):
+            cols = slice(n * wide, (n + 1) * wide)
+            part[half_of(h), cols] = dot(c_out[half_of(h), :], woc[:, cols])
+
+    conv_half(yo)
+    attend([sp], yo, True)
+    conv_half(y)
+    attend([sp], y, True)
+    loaded(10, 11)
+    close_conv(yo)
+    loaded(11, 12)
+    out_conv(yo)
     relay_kv(yo)
 
     @pl.when(lane == 1)
     def _():
         arrived(sp - 1, y)
         arrived(sp - 1, yo)
-
-        def partner_block(q, c):
-            attend([sp - 1], q, False)
-            return c
-
-        lax.fori_loop(0, 2, partner_block, 0)
-
-    for i in range(1, tp_n):
-        stat_copy(i).wait_recv()
-    sums = stat[0]
-    for i in range(1, tp_n):
-        sums = sums + stat[i]
-    sums = sums / (chans * tp_n)
-    mu = sums[0:1]
-    inv = lax.rsqrt(sums[1:2] - mu * mu + 1e-05)
-    mu_t = jnp.broadcast_to(mu, (128, tok)).T
-    inv_t = jnp.broadcast_to(inv, (128, tok)).T
-    for cc in range(0, chans, 128):
-        val = (conv[:, cc : cc + 128] - mu_t) * inv_t * ln_gain[:, cc : cc + 128]
-        c_out[:, cc : cc + 128] = (val * jax.nn.sigmoid(val)).astype(BF16)
-    loads[5].wait()
-    wide = y_s.shape[2]
-    chunks = width // wide
-
-    def out_conv(n, c):
-        cols = pl.ds(pl.multiple_of(n * wide, wide), wide)
-        part[:, cols] = dot(c_out[...], woc[:, cols])
-        return c
-
-    lax.fori_loop(0, chunks, out_conv, 0)
+        attend([sp - 1], yo, False)
+        attend([sp - 1], y, False)
+
+    close_conv(y)
+    out_conv(y)
 
     def pairs(q, first):
         def one(i, c):
@@ -451,6 +460,7 @@
 
         lax.fori_loop(0, pos, one, 0)
 
+    loaded(12, 15)
     sub_t = jnp.broadcast_to(sub_gain[...], (half_rows, vdim)).T
 
     def close_heads(q):
@@ -465,8 +475,6 @@
             out = diff * lax.rsqrt(jnp.mean(diff * diff, axis=0, keepdims=True) + 1e-06) * sub_t
             a_out[at, h * vdim : (h + 1) * vdim] = out.T.astype(BF16)
 
-    loads[6].wait()
-
     def mate_copy(k, n):
         return pltpu.make_async_remote_copy(
             src_ref=mate_s.at[k, n],
@@ -487,21 +495,18 @@
             device_id_type=MESH,
         )
 
-    def half_of(h):
-        return pl.ds(pl.multiple_of(h * half_rows, half_rows), half_rows)
-
     def owner_rows(h, c):
         return pl.ds(pl.multiple_of((h * 2 + c) * rows, rows), rows)
 
     def out_attn(k, h):
-        def one(n, c):
-            cols = pl.ds(pl.multiple_of(n * wide, wide), wide)
-            part[half_of(h), cols] += dot(a_out[half_of(h), :], woa[:, cols])
-            mate_s[k, n] = part[owner_rows(h, 1 - core), cols].astype(BF16)
-            mate_copy(k, n).start()
-            return c
-
-        lax.fori_loop(0, chunks, one, 0)
+        for piece in (range(0, 1), range(1, chunks)):
+            for n in piece:
+                cols = slice(n * wide, (n + 1) * wide)
+                part[half_of(h), cols] += dot(a_out[half_of(h), :], woa[:, cols])
+            for n in piece:
+                cols = slice(n * wide, (n + 1) * wide)
+                mate_s[k, n] = part[owner_rows(h, 1 - core), cols].astype(BF16)
+                mate_copy(k, n).start()
 
     pairs(yo, True)
     close_heads(yo)
@@ -531,8 +536,9 @@
 
     for copy in ag_cross + ag_mate + ag_fwd:
         copy.wait_send()
-    for i in range(1, tp_n):
-        stat_copy(i).wait_send()
+    for h in range(2):
+        for i in range(1, tp_n):
+            stat_copy(h, i).wait_send()
 
     @pl.when(sp < sp_n - 1)
     def _():
@@ -635,12 +641,12 @@
             pltpu.VMEM((tp_n, rows, width), BF16),
             pltpu.VMEM((sp_n, 2, half + vcols, half), BF16),
             pltpu.VMEM((2, kcols, heads * tok), BF16),
-            pltpu.VMEM((HALO + tok, chans), F32),
+            pltpu.VMEM((chans // 128, HALO + tok, 128), F32),
             pltpu.VMEM((HALO, chans), BF16),
             pltpu.VMEM((HALO, chans), BF16),
-            pltpu.VMEM((tok, chans), F32),
-            pltpu.VMEM((2, tok, 128), F32),
-            pltpu.VMEM((tp_n, 2, tok), F32),
+            pltpu.VMEM((chans // 128, tok, 128), F32),
+            pltpu.VMEM((2, half, 128), F32),
+            pltpu.VMEM((2, tp_n, 2, half), F32),
             pltpu.VMEM((tok, chans), BF16),
             [pltpu.VMEM((2, 1, tok), F32) for _ in range(heads)],
             [pltpu.VMEM((2, 1, tok), F32) for _ in range(heads)],
@@ -651,16 +657,15 @@
             pltpu.VMEM((2, chunks, rows, wide), BF16),
             pltpu.VMEM((chunks, rows, wide), BF16),
             pltpu.VMEM((chunks, rows, wide), BF16),
-            dma((8,)),
-            dma((7,)),
+            dma((15,)),
             dma((3, 4)),
             dma((3, 4)),
             dma((sp_n // 2, 2)),
             dma((sp_n // 2, 2)),
             dma((sp_n, 2)),
             dma((2,)),
-            dma((tp_n,)),
-            dma((tp_n,)),
+            dma((2, tp_n)),
+            dma((2, tp_n)),
             dma((2, chunks)),
             dma((2, chunks)),
             dma((chunks,)),

time: 41.2 us -> 37.1 us (0.900)
  Pallas kernels: 39.9 us -> 36 us
    pallas_call x1, Pallas kernels: 39.1 us -> 35.3 us  [on_device(): pl.pallas_call(functools.partial(kernel, sp_n, tp_n), out_shape=(pltpu.VM...]
where the time goes in v2:
time: 37.1 us; the launch traced here: 36.7 us
  Pallas kernels  36 us (97%)
  between operations  0.64 us (2%)
    pallas_call x1, Pallas kernels, on_device(): pl.pallas_call(functools.partial(kernel, sp_n, tp_n), out_shape=(pltpu.VM...  35.3 us

profile of v2, /device:TPU:25, one launch (start us, length us, event | category | flops | bytes accessed | tf_op | source)
XLA Modules:
  0.0 36.7 jit_solution(10710366106270788720)
XLA Ops:
  0.6 35.3 %shard_map.158 = (bf16[64,2048]{1,0:T(8,128)(2,1)S(1)}, f32[2,4,256]{2,1,0:T(4,128)S(1)}) custom-call(bf16[64,2048]{1,0:T(8,128)(2,1)} %tokens_hbm.1, f32[1,2048]{1,0:T(1,128)} %bitcast.3, bf16[2048,512]{1,0:T(8,128)(2,1)} %w_glu_a.1, bf16[2048,512]{1,0:T(8,128)(2,1)} %w_glu_b.1, f32[31,512]{1,0:T(8,128)} %taps_hbm.1, f32[1,512]{1,0:T(1,128)} %bitcast.4, ...), custom_call_target="tpu_custom_call" | custom-call | tf_op jit(solution)/shard_map/pallas_call | solution.py:618
  35.9 0.7 %shard_map.159 = (bf16[64,2048]{1,0:T(8,128)(2,1)}, f32[2,4,256]{2,1,0:T(4,128)}) custom-call(bf16[64,2048]{1,0:T(8,128)(2,1)S(1)} %get-tuple-element.4.mixed, f32[2,4,256]{2,1,0:T(4,128)S(1)} %get-tuple-element.5.logs), custom_call_target="tpu_custom_call" | custom-call | tf_op jit(solution)/shard_map/pallas_call | solution.py:694

commit v3 on v2

--- a/solution.py
+++ b/solution.py
@@ -9,6 +9,8 @@
 
 KW = 31
 HALO = 32
+LOG2_E = 1.4426950408889634
+LN_2 = 0.6931471805599453
 F32 = jnp.float32
 BF16 = jnp.bfloat16
 MESH = pl.DeviceIdType.MESH
@@ -155,7 +157,7 @@
     ag_chunks = 4
 
     def ag_copy(slot, k, i, target):
-        piece = pl.ds(i * (rows // ag_chunks), rows // ag_chunks)
+        piece = pl.ds((ag_chunks - 1 - i) * (rows // ag_chunks), rows // ag_chunks)
         return pltpu.make_async_remote_copy(
             src_ref=nrm.at[slot, piece],
             dst_ref=nrm.at[slot, piece],
@@ -183,90 +185,156 @@
     def half_in(h):
         return nrm[pl.ds(2 * h, 2)].reshape(half_rows, width)
 
-    def proj_kv(h):
-        res = dot(half_in(h), wkv[...])
+    def norm_kv(xin):
+        res = dot(xin, wkv[...])
         k = res[:, :kw]
-        v = res[:, kw:]
         first = lax.broadcasted_iota(jnp.int32, k.shape, 1) < hd
         sq = k * k
         s0 = jnp.sum(jnp.where(first, sq, 0.0), axis=1, keepdims=True)
         s1 = jnp.sum(jnp.where(first, 0.0, sq), axis=1, keepdims=True)
         r = jnp.where(first, lax.rsqrt(s0 / hd + 1e-06), lax.rsqrt(s1 / hd + 1e-06))
-        kv[sp, h, :half_rows, :] = (k * r * k_gain[...]).astype(BF16)
-        kv[sp, h, half_rows:, :] = v.T.astype(BF16)
-
-    def z_copy(t, h):
-        return pltpu.make_async_remote_copy(
-            src_ref=kv.at[sp, h],
-            dst_ref=kv.at[sp, h],
-            send_sem=z_send.at[t, h],
-            recv_sem=kv_recv.at[sp, h],
-            device_id=(t * 2 + lane, tp),
-            device_id_type=MESH,
-        )
-
-    def x_copy(p, h):
+        return (k * r * k_gain[...]).astype(BF16), res[:, kw:].astype(BF16)
+
+    half_slot = rows // 2
+
+    def first_row(i):
+        return (1 - i) * half_slot
+
+    def unit_in(i):
+        at = slice(first_row(i), first_row(i) + half_slot)
+        return jnp.concatenate([nrm[2 * yo, at, :], nrm[2 * yo + 1, at, :]], axis=0)
+
+    def proj_kv_near():
+        k, v = norm_kv(half_in(y))
+        for i in range(2):
+            for j in range(2):
+                src = slice(j * rows + first_row(i), j * rows + first_row(i) + half_slot)
+                dst = slice(j * half_slot, (j + 1) * half_slot)
+                kv[sp, 2 * y + i, dst, :] = k[src]
+                kv[sp, 2 * y + i, rows + j * half_slot : rows + (j + 1) * half_slot, :] = v[src]
+
+    def proj_kv_far(i):
+        k, v = norm_kv(unit_in(i))
+        kv[sp, 2 * yo + i, :rows, :] = k
+        kv[sp, 2 * yo + i, rows:, :] = v
+
+    def kv_part(s, m):
+        if m == 0:
+            return kv.at[s, pl.ds(2 * y, 2)]
+        return kv.at[s, pl.ds(2 * yo + m - 1, 1)]
+
+    def z_copy(p, m, d):
         s = p * 2 + lane
         return pltpu.make_async_remote_copy(
-            src_ref=kv.at[s, h],
-            dst_ref=kv.at[s, h],
-            send_sem=x_send.at[p, h],
-            recv_sem=kv_recv.at[s, h],
+            src_ref=kv_part(s, m),
+            dst_ref=kv_part(s, m),
+            send_sem=z_send.at[p, m, d - 1],
+            recv_sem=kv_recv.at[s, m],
+            device_id=((pos + d) * 2 + lane, tp),
+            device_id_type=MESH,
+        )
+
+    last = pos == npos - 1
+
+    def x_copy(p, m):
+        s = p * 2 + lane
+        return pltpu.make_async_remote_copy(
+            src_ref=kv_part(s, m),
+            dst_ref=kv_part(s, m),
+            send_sem=x_send.at[p, m],
+            recv_sem=kv_recv.at[s, m],
             device_id=(xmate, tp),
             device_id_type=MESH,
         )
 
-    def arrived(s, h):
+    def arrived(s, m):
         pltpu.make_async_remote_copy(
-            src_ref=kv.at[s, h],
-            dst_ref=kv.at[s, h],
-            send_sem=x_send.at[0, h],
-            recv_sem=kv_recv.at[s, h],
+            src_ref=kv_part(s, m),
+            dst_ref=kv_part(s, m),
+            send_sem=x_send.at[0, m],
+            recv_sem=kv_recv.at[s, m],
             device_id=(xmate, tp),
             device_id_type=MESH,
         ).wait_recv()
 
-    def send_kv(h):
+    late = 2
+
+    def direct_kv(then):
+        def one(i, c):
+            then(z_copy(pos, late, npos - 1 - pos - i))
+            return c
+
+        lax.fori_loop(0, npos - 1 - pos, one, 0)
+
+    def tree_kv(p, m, then):
+        @pl.when((p == pos) & (pos + 2 < npos))
+        def _():
+            then(z_copy(p, m, 2))
+
+        @pl.when((p != pos - 1) & (pos + 1 < npos))
+        def _():
+            then(z_copy(p, m, 1))
+
+    def send_kv(m):
+        if m == late:
+            direct_kv(lambda copy: copy.start())
+        else:
+            tree_kv(pos, m, lambda copy: copy.start())
+
         @pl.when(lane == 0)
         def _():
-            x_copy(pos, h).start()
-
-        def one(i, c):
-            z_copy(npos - 1 - i, h).start()
-            return c
-
-        lax.fori_loop(0, npos - 1 - pos, one, 0)
-
-    def relay_kv(h):
+            x_copy(pos, m).start()
+
+    def relay_kv(m, lo, hi=None):
         def one(i, c):
             p = pos - 1 - i
-            arrived(p * 2 + lane, h)
-            x_copy(p, h).start()
+            arrived(p * 2 + lane, m)
+            if m != late:
+                tree_kv(p, m, lambda copy: copy.start())
+            x_copy(p, m).start()
             return c
 
-        lax.fori_loop(0, pos, one, 0)
-
-    def proj_glu(h):
-        xin = half_in(h)
+        lax.fori_loop(lo, pos if hi is None else jnp.minimum(pos, hi), one, 0)
+
+    def relay_last(m, lo, hi):
+        relay_kv(m, lo, jnp.where(last, hi, 0))
+
+    def relay_rest(m, lo, hi):
+        relay_kv(m, lo, jnp.where(last, 0, hi))
+
+    def gate(xin, n):
         wide = 256
-
-        def one(n, c):
-            cols = pl.ds(pl.multiple_of(n * wide, wide), wide)
-            a = dot(xin, wa[:, cols])
-            b = dot(xin, wb[:, cols])
-            g = (a * jax.nn.sigmoid(b)).astype(BF16)
-            at = pl.ds(pl.multiple_of(HALO + h * half_rows, HALO), half_rows)
-            for j in range(wide // 128):
-                gat[n * (wide // 128) + j, at, :] = g[:, j * 128 : (j + 1) * 128].astype(F32)
-
-            @pl.when(h == 1)
+        cols = slice(n * wide, (n + 1) * wide)
+        a = dot(xin, wa[:, cols])
+        b = dot(xin, wb[:, cols])
+        return (a * jax.nn.sigmoid(b)).astype(BF16)
+
+    def proj_glu_near():
+        xin = half_in(y)
+        at = pl.ds(pl.multiple_of(HALO + y * half_rows, HALO), half_rows)
+        for n in range(chans // 256):
+            g = gate(xin, n)
+            for j in range(2):
+                gat[2 * n + j, at, :] = g[:, j * 128 : (j + 1) * 128].astype(F32)
+
+            @pl.when(y == 1)
             def _():
-                halo_s[:, cols] = g[half_rows - HALO :, :]
-
-            return c
-
-        for n in range(chans // wide):
-            one(n, 0)
+                halo_s[:, n * 256 : (n + 1) * 256] = g[half_rows - HALO :, :]
+
+    def proj_glu_far(i):
+        xin = unit_in(i)
+        for n in range(chans // 256):
+            g = gate(xin, n)
+            for t in range(2):
+                at = pl.ds(pl.multiple_of(HALO + yo * half_rows + t * rows + first_row(i), HALO), half_slot)
+                part_g = g[t * half_slot : (t + 1) * half_slot]
+                for j in range(2):
+                    gat[2 * n + j, at, :] = part_g[:, j * 128 : (j + 1) * 128].astype(F32)
+            if i == 0:
+
+                @pl.when(yo == 1)
+                def _():
+                    halo_s[:, n * 256 : (n + 1) * 256] = g[rows - HALO : rows, :]
 
     def proj_q(h):
         xin = half_in(h)
@@ -280,10 +348,13 @@
                 gain = jnp.broadcast_to(q_gain[pl.ds(n * 2 + j, 1), :], (2 * hd, 2 * hd)).T
                 for m in range(2):
                     gm = gain[m * hd : (m + 1) * hd, :half_rows]
-                    val = (qn[j * 2 + m] * gm * hd ** (-0.5)).astype(BF16)
+                    val = (qn[j * 2 + m] * gm).astype(BF16).astype(F32) * (hd ** (-0.5) * LOG2_E)
+                    high = val.astype(BF16)
+                    low = (val - high.astype(F32)).astype(BF16)
                     first = (n * 2 + j) * tok + m * half_rows
                     lanes = pl.ds(pl.multiple_of(first, half_rows), half_rows)
-                    qtz[h, m * hd : (m + 1) * hd, lanes] = val
+                    qtz[h, m * hd : (m + 1) * hd, lanes] = high
+                    qtz[h, (m + 2) * hd : (m + 3) * hd, lanes] = low
             return c
 
         for n in range(heads // 2):
@@ -306,51 +377,67 @@
 
     loaded(2, 5)
     ag_mate[0].wait_recv()
-    proj_kv(y)
-    send_kv(y)
+    proj_kv_near()
+    send_kv(0)
     loaded(5, 7)
-    proj_glu(y)
+    proj_glu_near()
     send_halo(y)
     loaded(7, 9)
     proj_q(y)
-    for i in range(ag_chunks):
-        ag_cross[i].wait_recv()
-        ag_fwd[i].start()
-    for i in range(ag_chunks):
-        ag_fwd[i].wait_recv()
-    proj_glu(yo)
+
+    def far_row(n):
+        ag_cross[n].wait_recv()
+        ag_fwd[n].start()
+
+    far_row(0)
+    far_row(1)
+    ag_fwd[0].wait_recv()
+    ag_fwd[1].wait_recv()
+    proj_kv_far(0)
+    send_kv(1)
+    far_row(2)
+
+    @pl.when(core == 1)
+    def _():
+        far_row(3)
+
+    proj_glu_far(0)
     send_halo(yo)
-    proj_kv(yo)
-    send_kv(yo)
-    relay_kv(y)
-    proj_q(yo)
-
-    def attend(blocks, q, diag):
-        keys = jnp.concatenate(
-            [kv[s, i, :half_rows, :] for s in blocks for i in range(2)], axis=0
-        )
-        vals = jnp.concatenate(
-            [kv[s, i, half_rows:, :] for s in blocks for i in range(2)], axis=1
-        )
+    @pl.when(core == 0)
+    def _():
+        far_row(3)
+
+    relay_rest(0, 0, npos)
+    relay_last(0, 0, 2)
+    ag_fwd[2].wait_recv()
+    ag_fwd[3].wait_recv()
+    proj_kv_far(1)
+    send_kv(2)
+    proj_glu_far(1)
+    def attend(blocks, q, diag, units=(0, 1, 2, 3)):
+        keys = jnp.concatenate([kv[s, u, :rows, :] for s in blocks for u in units], axis=0)
+        vals = jnp.concatenate([kv[s, u, rows:, :] for s in blocks for u in units], axis=0).T
         if diag:
-            kpos = lax.broadcasted_iota(jnp.int32, (tok, tok), 0)
-            qpos = lax.broadcasted_iota(jnp.int32, (tok, tok), 1)
+            e = lax.broadcasted_iota(jnp.int32, (tok, 1), 0)
+            kpos = e // half_rows * half_rows + e // half_slot % 2 * rows
+            kpos = kpos + (1 - e // rows % 2) * half_slot + e % half_slot
+            qpos = lax.broadcasted_iota(jnp.int32, (1, tok), 1)
             qpos = jnp.where(qpos >= half_rows, qpos - half_rows, qpos) + q * half_rows
             seen = kpos <= qpos
-        every = dot(keys, qtz[q])
+        every = dot(jnp.concatenate([keys, keys], axis=1), qtz[q])
         for h in range(heads):
             sc = every[:, h * tok : (h + 1) * tok]
             if diag:
                 sc = jnp.where(seen, sc, -1e30)
                 top = jnp.max(sc, axis=0, keepdims=True)
-                wgt = jnp.exp(sc - top)
+                wgt = jnp.exp2(sc - top)
                 l_ref[h][q] = jnp.sum(wgt, axis=0, keepdims=True)
                 acc[h][q] = dot(vals, wgt.astype(BF16))
             else:
                 old = m_ref[h][q]
                 top = jnp.maximum(old, jnp.max(sc, axis=0, keepdims=True))
-                wgt = jnp.exp(sc - top)
-                alpha = jnp.exp(old - top)
+                wgt = jnp.exp2(sc - top)
+                alpha = jnp.exp2(old - top)
                 l_ref[h][q] = l_ref[h][q] * alpha + jnp.sum(wgt, axis=0, keepdims=True)
                 acc[h][q] = acc[h][q] * alpha + dot(vals, wgt.astype(BF16))
             m_ref[h][q] = top
@@ -429,33 +516,62 @@
             cols = slice(n * wide, (n + 1) * wide)
             part[half_of(h), cols] = dot(c_out[half_of(h), :], woc[:, cols])
 
+    relay_rest(1, 0, 1)
     conv_half(yo)
+    relay_rest(1, 1, npos)
+    relay_last(1, 0, 2)
+    conv_half(y)
+    proj_q(yo)
     attend([sp], yo, True)
-    conv_half(y)
-    attend([sp], y, True)
+    relay_rest(2, 0, 1)
+    relay_last(0, 2, npos)
+
+    @pl.when(lane == 1)
+    def _():
+        for m in range(3):
+            arrived(sp - 1, m)
+        attend([sp - 1], yo, False)
+
+    relay_rest(2, 1, npos)
+    relay_last(1, 2, npos)
+    relay_last(2, 0, 2)
     loaded(10, 11)
     close_conv(yo)
     loaded(11, 12)
     out_conv(yo)
-    relay_kv(yo)
-
-    @pl.when(lane == 1)
-    def _():
-        arrived(sp - 1, y)
-        arrived(sp - 1, yo)
-        attend([sp - 1], yo, False)
-        attend([sp - 1], y, False)
-
-    close_conv(y)
-    out_conv(y)
-
-    def pairs(q, first):
+    relay_last(2, 2, npos)
+    def near_part():
+        attend([sp], y, True)
+        close_conv(y)
+        out_conv(y)
+
+        @pl.when(lane == 1)
+        def _():
+            attend([sp - 1], y, False)
+
+    pl.when(pos > 0)(near_part)
+
+    def pairs_far():
+        def early(i, c):
+            p = pos - 1 - i
+            for m in range(2):
+                arrived(p * 2 + 1 - lane, m)
+            attend([p * 2, p * 2 + 1], yo, False, (2 * y, 2 * y + 1, 2 * yo))
+            return c
+
+        def late(i, c):
+            p = pos - 1 - i
+            arrived(p * 2 + 1 - lane, 2)
+            attend([p * 2, p * 2 + 1], yo, False, (2 * yo + 1,))
+            return c
+
+        lax.fori_loop(0, pos, early, 0)
+        lax.fori_loop(0, pos, late, 0)
+
+    def pairs_near():
         def one(i, c):
             p = pos - 1 - i
-            if first:
-                arrived(p * 2 + 1 - lane, y)
-                arrived(p * 2 + 1 - lane, yo)
-            attend([p * 2, p * 2 + 1], q, False)
+            attend([p * 2, p * 2 + 1], y, False)
             return c
 
         lax.fori_loop(0, pos, one, 0)
@@ -467,7 +583,7 @@
         at = pl.ds(pl.multiple_of(q * half_rows, half_rows), half_rows)
         for h in range(heads):
             total = l_ref[h][q]
-            log_row = m_ref[h][q] + jnp.log(total)
+            log_row = m_ref[h][q] * LN_2 + jnp.log(total)
             maps = acc[h][q] / total
             for m in range(2):
                 logs[m, h : h + 1, at] = log_row[:, m * half_rows : (m + 1) * half_rows]
@@ -508,9 +624,10 @@
                 mate_s[k, n] = part[owner_rows(h, 1 - core), cols].astype(BF16)
                 mate_copy(k, n).start()
 
-    pairs(yo, True)
+    pairs_far()
     close_heads(yo)
     out_attn(0, yo)
+    pl.when(pos == 0)(near_part)
 
     def forward(n, c):
         cols = pl.ds(pl.multiple_of(n * wide, wide), wide)
@@ -520,7 +637,7 @@
         return c
 
     lax.fori_loop(0, chunks, forward, 0)
-    pairs(y, False)
+    pairs_near()
     close_heads(y)
     out_attn(1, y)
 
@@ -544,23 +661,24 @@
     def _():
         halo_copy().wait_send()
 
-    for h in range(2):
+    for m in range(3):
 
         @pl.when(lane == 0)
         def _():
-            x_copy(pos, h).wait_send()
-
-        def z_done(i, c):
-            z_copy(npos - 1 - i, h).wait_send()
+            x_copy(pos, m).wait_send()
+
+        if m == late:
+            direct_kv(lambda copy: copy.wait_send())
+        else:
+            tree_kv(pos, m, lambda copy: copy.wait_send())
+
+        def relay_done(p, c):
+            x_copy(p, m).wait_send()
+            if m != late:
+                tree_kv(p, m, lambda copy: copy.wait_send())
             return c
 
-        lax.fori_loop(0, npos - 1 - pos, z_done, 0)
-
-        def x_done(i, c):
-            x_copy(i, h).wait_send()
-            return c
-
-        lax.fori_loop(0, pos, x_done, 0)
+        lax.fori_loop(0, pos, relay_done, 0)
 
     def rs_done(n, c):
         mate_copy(0, n).wait_send()
@@ -639,8 +757,8 @@
             pltpu.VMEM((chans, width), BF16),
             pltpu.VMEM((acols, width), BF16),
             pltpu.VMEM((tp_n, rows, width), BF16),
-            pltpu.VMEM((sp_n, 2, half + vcols, half), BF16),
-            pltpu.VMEM((2, kcols, heads * tok), BF16),
+            pltpu.VMEM((sp_n, 4, 2 * rows, kcols), BF16),
+            pltpu.VMEM((2, 2 * kcols, heads * tok), BF16),
             pltpu.VMEM((chans // 128, HALO + tok, 128), F32),
             pltpu.VMEM((HALO, chans), BF16),
             pltpu.VMEM((HALO, chans), BF16),
@@ -660,9 +778,9 @@
             dma((15,)),
             dma((3, 4)),
             dma((3, 4)),
-            dma((sp_n // 2, 2)),
-            dma((sp_n // 2, 2)),
-            dma((sp_n, 2)),
+            dma((sp_n // 2, 3, max(2, sp_n // 2 - 1))),
+            dma((sp_n // 2, 3)),
+            dma((sp_n, 3)),
             dma((2,)),
             dma((2, tp_n)),
             dma((2, tp_n)),

time: 37.1 us -> 35.2 us (0.949)
  Pallas kernels: 36 us -> 34.4 us
    pallas_call x1, Pallas kernels: 35.3 us -> 33.7 us  [on_device(): pl.pallas_call(functools.partial(kernel, sp_n, tp_n), out_shape=(pltpu.VM...]
where the time goes in v3:
time: 35.2 us; the launch traced here: 35.1 us
  Pallas kernels  34.4 us (98%)
  between operations  0.64 us (2%)
    pallas_call x1, Pallas kernels, on_device(): pl.pallas_call(functools.partial(kernel, sp_n, tp_n), out_shape=(pltpu.VM...  33.7 us
    pallas_call x1, Pallas kernels, on_device(): pl.pallas_call(put_out, out_shape=(jax.ShapeDtypeStruct((rows, width), BF...  0.72 us

profile of v3, /device:TPU:25, one launch (start us, length us, event | category | flops | bytes accessed | tf_op | source)
XLA Modules:
  0.0 35.1 jit_solution(14610848277025764587)
XLA Ops:
  0.6 33.7 %shard_map.158 = (bf16[64,2048]{1,0:T(8,128)(2,1)S(1)}, f32[2,4,256]{2,1,0:T(4,128)S(1)}) custom-call(bf16[64,2048]{1,0:T(8,128)(2,1)} %tokens_hbm.1, f32[1,2048]{1,0:T(1,128)} %bitcast.3, bf16[2048,512]{1,0:T(8,128)(2,1)} %w_glu_a.1, bf16[2048,512]{1,0:T(8,128)(2,1)} %w_glu_b.1, f32[31,512]{1,0:T(8,128)} %taps_hbm.1, f32[1,512]{1,0:T(1,128)} %bitcast.4, ...), custom_call_target="tpu_custom_call" | custom-call | tf_op jit(solution)/shard_map/pallas_call | solution.py:736
  34.3 0.7 %shard_map.159 = (bf16[64,2048]{1,0:T(8,128)(2,1)}, f32[2,4,256]{2,1,0:T(4,128)}) custom-call(bf16[64,2048]{1,0:T(8,128)(2,1)S(1)} %get-tuple-element.4.mixed, f32[2,4,256]{2,1,0:T(4,128)S(1)} %get-tuple-element.5.logs), custom_call_target="tpu_custom_call" | custom-call | tf_op jit(solution)/shard_map/pallas_call | solution.py:812

commit v4 on v3

--- a/solution.py
+++ b/solution.py
@@ -285,13 +285,15 @@
         def _():
             x_copy(pos, m).start()
 
-    def relay_kv(m, lo, hi=None):
+    def relay_kv(m, lo, hi=None, along=True, across=True):
         def one(i, c):
             p = pos - 1 - i
-            arrived(p * 2 + lane, m)
-            if m != late:
-                tree_kv(p, m, lambda copy: copy.start())
-            x_copy(p, m).start()
+            if along:
+                arrived(p * 2 + lane, m)
+                if m != late:
+                    tree_kv(p, m, lambda copy: copy.start())
+            if across:
+                x_copy(p, m).start()
             return c
 
         lax.fori_loop(lo, pos if hi is None else jnp.minimum(pos, hi), one, 0)
@@ -299,8 +301,8 @@
     def relay_last(m, lo, hi):
         relay_kv(m, lo, jnp.where(last, hi, 0))
 
-    def relay_rest(m, lo, hi):
-        relay_kv(m, lo, jnp.where(last, 0, hi))
+    def relay_rest(m, lo, hi, along=True, across=True):
+        relay_kv(m, lo, jnp.where(last, 0, hi), along, across)
 
     def gate(xin, n):
         wide = 256
@@ -395,6 +397,7 @@
     ag_fwd[1].wait_recv()
     proj_kv_far(0)
     send_kv(1)
+    relay_rest(0, 1, npos, across=False)
     far_row(2)
 
     @pl.when(core == 1)
@@ -407,7 +410,8 @@
     def _():
         far_row(3)
 
-    relay_rest(0, 0, npos)
+    relay_rest(0, 0, 1)
+    relay_rest(0, 1, npos, along=False)
     relay_last(0, 0, 2)
     ag_fwd[2].wait_recv()
     ag_fwd[3].wait_recv()
@@ -520,53 +524,65 @@
     conv_half(yo)
     relay_rest(1, 1, npos)
     relay_last(1, 0, 2)
-    conv_half(y)
+    tail = last & (lane == 0) & (pos > 0)
+
+    @pl.when(jnp.logical_not(tail))
+    def _():
+        conv_half(y)
+
+    relay_last(0, 2, npos)
     proj_q(yo)
     attend([sp], yo, True)
     relay_rest(2, 0, 1)
-    relay_last(0, 2, npos)
+    relay_last(2, 0, 1)
 
     @pl.when(lane == 1)
     def _():
         for m in range(3):
             arrived(sp - 1, m)
         attend([sp - 1], yo, False)
-
-    relay_rest(2, 1, npos)
-    relay_last(1, 2, npos)
-    relay_last(2, 0, 2)
-    loaded(10, 11)
-    close_conv(yo)
-    loaded(11, 12)
-    out_conv(yo)
-    relay_last(2, 2, npos)
-    def near_part():
+        relay_last(1, 2, npos)
+        relay_last(2, 1, 2)
+
+    def near_attn():
         attend([sp], y, True)
-        close_conv(y)
-        out_conv(y)
 
         @pl.when(lane == 1)
         def _():
             attend([sp - 1], y, False)
 
-    pl.when(pos > 0)(near_part)
+    def near_conv():
+        close_conv(y)
+        out_conv(y)
+
+    @pl.when(tail)
+    def _():
+        conv_half(y)
+
+    relay_rest(2, 1, npos)
+    pl.when(pos > 0)(near_attn)
+
+    @pl.when(lane == 0)
+    def _():
+        relay_last(1, 2, npos)
+        relay_last(2, 1, 2)
+
+    relay_last(2, 2, npos)
 
     def pairs_far():
-        def early(i, c):
+        def one(i, c):
             p = pos - 1 - i
-            for m in range(2):
+            for m in range(3):
                 arrived(p * 2 + 1 - lane, m)
-            attend([p * 2, p * 2 + 1], yo, False, (2 * y, 2 * y + 1, 2 * yo))
+            attend([p * 2, p * 2 + 1], yo, False)
             return c
 
-        def late(i, c):
-            p = pos - 1 - i
-            arrived(p * 2 + 1 - lane, 2)
-            attend([p * 2, p * 2 + 1], yo, False, (2 * yo + 1,))
-            return c
-
-        lax.fori_loop(0, pos, early, 0)
-        lax.fori_loop(0, pos, late, 0)
+        loaded(10, 11)
+        close_conv(yo)
+        loaded(11, 12)
+        out_conv(yo)
+        pl.when((pos > 0) & jnp.logical_not(tail))(near_conv)
+        lax.fori_loop(0, pos, one, 0)
 
     def pairs_near():
         def one(i, c):
@@ -627,7 +643,6 @@
     pairs_far()
     close_heads(yo)
     out_attn(0, yo)
-    pl.when(pos == 0)(near_part)
 
     def forward(n, c):
         cols = pl.ds(pl.multiple_of(n * wide, wide), wide)
@@ -637,6 +652,13 @@
         return c
 
     lax.fori_loop(0, chunks, forward, 0)
+
+    @pl.when(pos == 0)
+    def _():
+        near_attn()
+
+    pl.when((pos == 0) | tail)(near_conv)
+
     pairs_near()
     close_heads(y)
     out_attn(1, y)
@@ -649,8 +671,6 @@
         mixed[:, cols] = total.astype(BF16)
         return c
 
-    lax.fori_loop(0, chunks, finish, 0)
-
     for copy in ag_cross + ag_mate + ag_fwd:
         copy.wait_send()
     for h in range(2):
@@ -679,6 +699,7 @@
             return c
 
         lax.fori_loop(0, pos, relay_done, 0)
+    lax.fori_loop(0, chunks, finish, 0)
 
     def rs_done(n, c):
         mate_copy(0, n).wait_send()

time: 35.2 us -> 34.6 us (0.983); the launches traced: 35.1 us -> 34 us
  Pallas kernels: 34.4 us -> 33.4 us
    pallas_call x1, Pallas kernels: 33.7 us -> 32.7 us  [on_device(): pl.pallas_call(functools.partial(kernel, sp_n, tp_n), out_shape=(pltpu.VM...]
where the time goes in v4:
time: 34.6 us; the launch traced here: 34 us
  Pallas kernels  33.4 us (97%)
  between operations  0.64 us (2%)
    pallas_call x1, Pallas kernels, on_device(): pl.pallas_call(functools.partial(kernel, sp_n, tp_n), out_shape=(pltpu.VM...  32.7 us
    pallas_call x1, Pallas kernels, on_device(): pl.pallas_call(put_out, out_shape=(jax.ShapeDtypeStruct((rows, width), BF...  0.72 us

profile of v4, /device:TPU:25, one launch (start us, length us, event | category | flops | bytes accessed | tf_op | source)
XLA Modules:
  0.0 34.0 jit_solution(568492400852151362)
XLA Ops:
  0.6 32.7 %shard_map.158 = (bf16[64,2048]{1,0:T(8,128)(2,1)S(1)}, f32[2,4,256]{2,1,0:T(4,128)S(1)}) custom-call(bf16[64,2048]{1,0:T(8,128)(2,1)} %tokens_hbm.1, f32[1,2048]{1,0:T(1,128)} %bitcast.3, bf16[2048,512]{1,0:T(8,128)(2,1)} %w_glu_a.1, bf16[2048,512]{1,0:T(8,128)(2,1)} %w_glu_b.1, f32[31,512]{1,0:T(8,128)} %taps_hbm.1, f32[1,512]{1,0:T(1,128)} %bitcast.4, ...), custom_call_target="tpu_custom_call" | custom-call | tf_op jit(solution)/shard_map/pallas_call | solution.py:757
  33.3 0.7 %shard_map.159 = (bf16[64,2048]{1,0:T(8,128)(2,1)}, f32[2,4,256]{2,1,0:T(4,128)}) custom-call(bf16[64,2048]{1,0:T(8,128)(2,1)S(1)} %get-tuple-element.4.mixed, f32[2,4,256]{2,1,0:T(4,128)S(1)} %get-tuple-element.5.logs), custom_call_target="tpu_custom_call" | custom-call | tf_op jit(solution)/shard_map/pallas_call | solution.py:833

commit v5 on v4

--- a/solution.py
+++ b/solution.py
@@ -179,7 +179,7 @@
         )
     ]
     ag_fwd = [ag_copy(cross, 2, i, mate) for i in range(ag_chunks)]
-    for copy in ag_cross + ag_mate:
+    for copy in ag_cross[:2] + ag_mate:
         copy.start()
 
     def half_in(h):
@@ -380,6 +380,8 @@
     loaded(2, 5)
     ag_mate[0].wait_recv()
     proj_kv_near()
+    for copy in ag_cross[2:]:
+        copy.start()
     send_kv(0)
     loaded(5, 7)
     proj_glu_near()
@@ -397,6 +399,7 @@
     ag_fwd[1].wait_recv()
     proj_kv_far(0)
     send_kv(1)
+    relay_last(0, 0, 1)
     relay_rest(0, 1, npos, across=False)
     far_row(2)
 
@@ -412,7 +415,7 @@
 
     relay_rest(0, 0, 1)
     relay_rest(0, 1, npos, along=False)
-    relay_last(0, 0, 2)
+    relay_last(0, 1, 2)
     ag_fwd[2].wait_recv()
     ag_fwd[3].wait_recv()
     proj_kv_far(1)
@@ -520,10 +523,10 @@
             cols = slice(n * wide, (n + 1) * wide)
             part[half_of(h), cols] = dot(c_out[half_of(h), :], woc[:, cols])
 
-    relay_rest(1, 0, 1)
+    relay_rest(1, 0, npos)
+    relay_last(1, 0, 1)
     conv_half(yo)
-    relay_rest(1, 1, npos)
-    relay_last(1, 0, 2)
+    relay_last(1, 1, 2)
     tail = last & (lane == 0) & (pos > 0)
 
     @pl.when(jnp.logical_not(tail))
@@ -542,7 +545,7 @@
             arrived(sp - 1, m)
         attend([sp - 1], yo, False)
         relay_last(1, 2, npos)
-        relay_last(2, 1, 2)
+        relay_last(2, 1, npos)
 
     def near_attn():
         attend([sp], y, True)
@@ -560,14 +563,13 @@
         conv_half(y)
 
     relay_rest(2, 1, npos)
-    pl.when(pos > 0)(near_attn)
-
     @pl.when(lane == 0)
     def _():
         relay_last(1, 2, npos)
-        relay_last(2, 1, 2)
-
-    relay_last(2, 2, npos)
+        relay_last(2, 1, npos)
+
+    pl.when(pos > 0)(near_attn)
+
 
     def pairs_far():
         def one(i, c):
@@ -577,12 +579,13 @@
             attend([p * 2, p * 2 + 1], yo, False)
             return c
 
+        ahead = jnp.where(tail, 1, 0)
+        lax.fori_loop(0, ahead, one, 0)
         loaded(10, 11)
         close_conv(yo)
         loaded(11, 12)
         out_conv(yo)
-        pl.when((pos > 0) & jnp.logical_not(tail))(near_conv)
-        lax.fori_loop(0, pos, one, 0)
+        lax.fori_loop(ahead, pos, one, 0)
 
     def pairs_near():
         def one(i, c):
@@ -657,7 +660,7 @@
     def _():
         near_attn()
 
-    pl.when((pos == 0) | tail)(near_conv)
+    near_conv()
 
     pairs_near()
     close_heads(y)

time: 34.6 us -> 34 us (0.983); the launches traced: 34 us -> 33.9 us
  no operation moved by 1% of the time
where the time goes in v5:
time: 34 us; the launch traced here: 33.9 us
  Pallas kernels  33.2 us (98%)
  between operations  0.64 us (2%)
    pallas_call x1, Pallas kernels, on_device(): pl.pallas_call(functools.partial(kernel, sp_n, tp_n), out_shape=(pltpu.VM...  32.5 us
    pallas_call x1, Pallas kernels, on_device(): pl.pallas_call(put_out, out_shape=(jax.ShapeDtypeStruct((rows, width), BF...  0.72 us

profile of v5, /device:TPU:25, one launch (start us, length us, event | category | flops | bytes accessed | tf_op | source)
XLA Modules:
  0.0 33.9 jit_solution(12455828198142096606)
XLA Ops:
  0.6 32.5 %shard_map.158 = (bf16[64,2048]{1,0:T(8,128)(2,1)S(1)}, f32[2,4,256]{2,1,0:T(4,128)S(1)}) custom-call(bf16[64,2048]{1,0:T(8,128)(2,1)} %tokens_hbm.1, f32[1,2048]{1,0:T(1,128)} %bitcast.3, bf16[2048,512]{1,0:T(8,128)(2,1)} %w_glu_a.1, bf16[2048,512]{1,0:T(8,128)(2,1)} %w_glu_b.1, f32[31,512]{1,0:T(8,128)} %taps_hbm.1, f32[1,512]{1,0:T(1,128)} %bitcast.4, ...), custom_call_target="tpu_custom_call" | custom-call | tf_op jit(solution)/shard_map/pallas_call | solution.py:760
  33.1 0.7 %shard_map.159 = (bf16[64,2048]{1,0:T(8,128)(2,1)}, f32[2,4,256]{2,1,0:T(4,128)}) custom-call(bf16[64,2048]{1,0:T(8,128)(2,1)S(1)} %get-tuple-element.4.mixed, f32[2,4,256]{2,1,0:T(4,128)S(1)} %get-tuple-element.5.logs), custom_call_target="tpu_custom_call" | custom-call | tf_op jit(solution)/shard_map/pallas_call | solution.py:836
